TPU v7x, 32 devices: a whole 2x2x4 slice. The times are simulated.
32 devices in a mesh: ep: 32 (over z, y, x, core).
Axes of the slice: x: 2, y: 2, z: 4, core: 2. Of those that a mesh axis runs over, the one named last changes fastest.
Arguments:
- tokens: bfloat16 [2048, 2048], P('ep'), may hold values from -6 to 6
- conv_state: bfloat16 [2048, 3, 1024], P('ep'), may hold values from -6 to 6
- recur_state: float32 [2048, 1024], P('ep'), may hold values from -6 to 6
- w_branch: bfloat16 [2048, 1024], replicated, may hold values from -0.125 to 0.125
- w_gate: bfloat16 [2048, 1024], replicated, may hold values from -0.125 to 0.125
- conv_taps: float32 [4, 1024], replicated, may hold values from -3 to 3
- rate_blocks: bfloat16 [16, 64, 64], replicated, may hold values from -0.75 to 0.75
- input_blocks: bfloat16 [16, 64, 64], replicated, may hold values from -0.75 to 0.75
- decay_param: float32 [1024], replicated, may hold values from 1.5 to 6.5
- w_mix: bfloat16 [1024, 2048], replicated, may hold values from -0.1875 to 0.1875
- gain_pre: float32 [2048], replicated, may hold values from 0.1 to 1.9
- gain_post: float32 [2048], replicated, may hold values from 0.1 to 1.9
- gain_ffn: float32 [2048], replicated, may hold values from 0.1 to 1.9
- gain_out: float32 [2048], replicated, may hold values from 0.1 to 1.9
- routes: int32 [2048, 2], P('ep'), may hold values from 0 to 31, all different within a row; in each aligned block of 64 rows (0 to 63, 64 to 127, ...) at most 12 rows name the same one
- affinity: float32 [2048, 2], P('ep'), may hold values from 0.05 to 1
- w_expert_gate: bfloat16 [32, 2048, 512], P('ep'), may hold values from -0.125 to 0.125
- w_expert_up: bfloat16 [32, 2048, 512], P('ep'), may hold values from -0.125 to 0.125
- w_expert_down: bfloat16 [32, 512, 2048], P('ep'), may hold values from -0.25 to 0.25
Outputs:
- layer_out: bfloat16 [2048, 2048], P('ep')
- conv_next: bfloat16 [2048, 3, 1024], P('ep')
- state_next: float32 [2048, 1024], P('ep')
Inputs may be any that keep to these rules, and one draw needn't show every extreme that they name: `routes`: each row names 2 different experts. Among the 64 rows of one device no expert is named more than 12 times, and in every draw some device names some expert exactly 12 times.
All inputs are finite; a program needn't handle non-finite values.
Results may differ from a plain program's by a relative error of at most 0.014.
Values may be sent and summed in bfloat16 or wider, within the bound.
A program may use at most 128 MiB of HBM per device.

v0:
```python
import jax
import jax.numpy as jnp
from jax import lax
from jax.sharding import PartitionSpec as P

epsilon = 1e-06
gate_scale = 8.0


def norm_rows(values, gain_vec):
    floats = values.astype(jnp.float32)
    inv_scale = lax.rsqrt(jnp.mean(floats * floats, axis=-1, keepdims=True) + epsilon)
    return floats * inv_scale * gain_vec


def recurrence(
    tokens,
    conv_state,
    recur_state,
    w_branch,
    w_gate,
    conv_taps,
    rate_blocks,
    input_blocks,
    decay_param,
    w_mix,
    gain_pre,
    gain_post,
):
    normed = norm_rows(tokens, gain_pre).astype(jnp.bfloat16)
    branch = jnp.dot(normed, w_branch, preferred_element_type=jnp.float32).astype(jnp.bfloat16)
    gate_act = jnp.dot(normed, w_gate, preferred_element_type=jnp.float32).astype(jnp.bfloat16)
    window = jnp.concatenate([conv_state, branch[:, None, :]], axis=1)
    convolved = jnp.sum(window.astype(jnp.float32) * conv_taps[None], axis=1)
    row_count, branch_width = convolved.shape
    blocks = rate_blocks.shape[0]
    pieces = convolved.reshape(row_count, blocks, branch_width // blocks)
    rate_gate = jax.nn.sigmoid(
        jnp.einsum("snc,ncd->snd", pieces, rate_blocks.astype(jnp.float32)).reshape(
            row_count, branch_width
        )
    )
    inflow = jax.nn.sigmoid(
        jnp.einsum("snc,ncd->snd", pieces, input_blocks.astype(jnp.float32)).reshape(
            row_count, branch_width
        )
    )
    log_decay = -gate_scale * rate_gate * jax.nn.softplus(-decay_param)
    state_next = jnp.exp(log_decay) * recur_state + jnp.sqrt(-jnp.expm1(2.0 * log_decay)) * (
        inflow * convolved
    )
    merged = (state_next * jax.nn.gelu(gate_act.astype(jnp.float32))).astype(jnp.bfloat16)
    mix_out = jnp.dot(merged, w_mix, preferred_element_type=jnp.float32).astype(jnp.bfloat16)
    residual = tokens.astype(jnp.float32) + norm_rows(mix_out, gain_post)
    return (residual, window[:, 1:, :], state_next)


def expert_block(got_rows, got_info, cap_total, w_expert_gate, w_expert_up, w_expert_down):
    slot_count, sources, model_width = got_rows.shape
    counts = got_info[0]
    before = jnp.cumsum(counts) - counts
    allowed = jnp.clip(cap_total - before, 0, counts)
    positions = jnp.arange(slot_count, dtype=jnp.int32)
    keep_mask = positions[:, None] < allowed[None, :]
    row_block = got_rows.reshape(slot_count * sources, model_width)
    gate_part = jnp.dot(row_block, w_expert_gate[0], preferred_element_type=jnp.float32)
    up_part = jnp.dot(row_block, w_expert_up[0], preferred_element_type=jnp.float32)
    hidden = (jax.nn.silu(gate_part) * up_part).astype(jnp.bfloat16)
    outputs = jnp.dot(hidden, w_expert_down[0], preferred_element_type=jnp.float32).astype(
        jnp.bfloat16
    )
    outputs = outputs.reshape(slot_count, sources, model_width)
    return jnp.where(keep_mask[:, :, None], outputs, jnp.zeros_like(outputs))


def shards(
    tokens,
    conv_state,
    recur_state,
    w_branch,
    w_gate,
    conv_taps,
    rate_blocks,
    input_blocks,
    decay_param,
    w_mix,
    gain_pre,
    gain_post,
    gain_ffn,
    gain_out,
    routes,
    affinity,
    w_expert_gate,
    w_expert_up,
    w_expert_down,
):
    residual, conv_next, state_next = recurrence(
        tokens,
        conv_state,
        recur_state,
        w_branch,
        w_gate,
        conv_taps,
        rate_blocks,
        input_blocks,
        decay_param,
        w_mix,
        gain_pre,
        gain_post,
    )
    ffn_in = norm_rows(residual, gain_ffn).astype(jnp.bfloat16)
    seq_count, top_count = routes.shape
    model_width = ffn_in.shape[1]
    experts = lax.axis_size("ep") * w_expert_gate.shape[0]
    capacity = max(2, 3 * seq_count * top_count // lax.axis_size("ep"))
    cap_total = seq_count * top_count // 2
    flat_routes = routes.reshape(-1)
    onehot = (flat_routes[:, None] == jnp.arange(experts, dtype=jnp.int32)[None, :]).astype(
        jnp.int32
    )
    slot_index = jnp.sum(jnp.cumsum(onehot, axis=0) * onehot, axis=1) - 1
    load_counts = jnp.sum(onehot, axis=0)
    slot_target = slot_index * experts + flat_routes
    outgoing = (
        jnp.zeros((capacity * experts, model_width), jnp.bfloat16)
        .at[slot_target]
        .set(jnp.repeat(ffn_in, top_count, axis=0))
    )
    outgoing = outgoing.reshape(capacity, experts, model_width)
    send_info = load_counts[None, :]
    got_rows, got_info = (
        lax.all_to_all(outgoing, "ep", split_axis=1, concat_axis=1, tiled=True),
        lax.all_to_all(send_info, "ep", split_axis=1, concat_axis=1, tiled=True),
    )
    finished = expert_block(
        got_rows, got_info, cap_total, w_expert_gate, w_expert_up, w_expert_down
    )
    gathered = lax.all_to_all(finished, "ep", split_axis=1, concat_axis=1, tiled=True)
    picked = jnp.take(gathered.reshape(capacity * experts, model_width), slot_target, axis=0)
    picked = picked.astype(jnp.float32).reshape(seq_count, top_count, model_width)
    weights = affinity / jnp.sum(affinity, axis=1, keepdims=True)
    combined = jnp.sum(weights[:, :, None] * picked, axis=1)
    layer_out = (residual + norm_rows(combined, gain_out)).astype(jnp.bfloat16)
    return (layer_out, conv_next, state_next)


def solution(mesh):
    return jax.shard_map(
        shards,
        mesh=mesh,
        in_specs=(
            P("ep", None),
            P("ep", None, None),
            P("ep", None),
            P(),
            P(),
            P(),
            P(),
            P(),
            P(),
            P(),
            P(),
            P(),
            P(),
            P(),
            P("ep", None),
            P("ep", None),
            P("ep", None, None),
            P("ep", None, None),
            P("ep", None, None),
        ),
        out_specs=(P("ep", None), P("ep", None, None), P("ep", None)),
        check_vma=False,
    )
```

profile of v0, /device:TPU:0, one launch (start us, length us, event | category | flops | bytes accessed | tf_op | source)
XLA Modules:
  0.0 170.9 jit_solution(7606808229073026035)
XLA Ops:
  0.6 0.9 copy.69
  1.6 0.1 eq.15
  1.8 0.2 reduce_window_sum.18
  2.0 0.7 fusion.55
  2.7 0.7 copy.72
  3.4 7.3 %all-to-all-start = ((s32[1,32,1]{2,0,1:T(1,128)}), s32[1,32,1]{2,0,1:T(1,128)S(1)}, u32[]{:S(2)}, u32[]{:S(2)}) async-start(s32[1,32,1]{2,0,1:T(1,128)} %copy.72), calls=%async_computation | async-start | bytes 32768 | tf_op jit(solution)/shard_map/all_to_all | solution.py:133
  10.7 0.7 reshape.196
  11.4 1.1 fusion.31
  12.5 3.2 %fusion.21 = bf16[64,1,1024]{2,0,1:T(8,128)(2,1)S(1)} fusion(bf16[2048,1024]{1,0:T(8,128)(2,1)} %param.22, bf16[64,2048]{1,0:T(8,128)(2,1)} %param.19, f32[2048]{0:T(1024)} %param.29, f32[64]{0:T(128)S(1)} %add_rsqrt_fusion.3), kind=kOutput, calls=%fused_computation.26 | convolution fusion | flops 269025280 | bytes 4595968 | tf_op jit(solution)/shard_map/dot_general | solution.py:31
  15.8 0.1 multiply_reduce_fusion.1
  15.9 0.2 reshape.193
  16.1 0.3 fusion.16
  16.4 0.3 copy.65
  16.7 0.2 div.38
  16.9 1.2 fusion.19
  18.2 0.3 copy.67
  18.5 0.9 div.40
  19.4 0.7 fusion.56
  20.1 1.3 multiply_add_fusion
  21.4 5.3 %multiply_reduce_fusion.4 = (f32[64]{0:T(128)S(1)}, f32[64,2048]{1,0:T(8,128)S(1)}) fusion(bf16[1024,2048]{1,0:T(8,128)(2,1)} %param.28, f32[64,1024]{1,0:T(8,128)S(1)} %multiply_add_fusion, bf16[2048,1024]{1,0:T(8,128)(2,1)} %param.23, bf16[64,2048]{1,0:T(8,128)(2,1)S(1)} %copy-done.1, f32[2048]{0:T(1024)} %param.29, f32[64]{0:T(128)} %copy-done.16), kind=kOutput, calls=%fused_computation.50 | convolution fusion | flops 538705856 | bytes 9445888 | tf_op jit(solution)/shard_map/dot_general | solution.py:53
  26.8 0.3 multiply_reduce_fusion.3
  27.1 0.2 multiply_convert_fusion
  27.3 0.5 fusion.57
  27.8 0.3 broadcast_in_dim.30
  28.1 1.0 reshape.214
  29.1 3.2 %scatter_custom_fusion = bf16[384,2048]{1,0:T(8,128)(2,1)} fusion(s32[128]{0:T(128)} %fusion.57, bf16[128,2048]{1,0:T(8,128)(2,1)} %reshape.214, bf16[]{:T(256)} %constant.60.clone.1), kind=kCustom, calls=%fused_computation.35 | custom fusion | bytes 1573376 | tf_op jit(solution)/shard_map/scatter | solution.py:127
  32.4 3.7 %copy.75 = bf16[12,32,2048]{2,0,1:T(8,128)(2,1)} copy(bf16[12,32,2048]{2,1,0:T(8,128)(2,1)} %bitcast.41) | data formatting | bytes 3145728 | tf_op jit(solution)/shard_map/reshape | solution.py:129
  36.0 6.1 %all-to-all-start.1 = ((bf16[12,32,2048]{2,0,1:T(8,128)(2,1)}), bf16[12,32,2048]{2,0,1:T(8,128)(2,1)}, u32[]{:S(2)}, u32[]{:S(2)}) async-start(bf16[12,32,2048]{2,0,1:T(8,128)(2,1)} %copy.75), calls=%async_computation.1 | async-start | bytes 4194304 | tf_op jit(solution)/shard_map/all_to_all | solution.py:132
  42.2 0.1 reduce.1
  42.4 0.7 reduce
  43.1 47.7 %all-to-all-done.1 = bf16[12,32,2048]{2,0,1:T(8,128)(2,1)} async-done(((bf16[12,32,2048]{2,0,1:T(8,128)(2,1)}), bf16[12,32,2048]{2,0,1:T(8,128)(2,1)}, u32[]{:S(2)}, u32[]{:S(2)}) %all-to-all-start.1) | async-done | bytes 1572896 | tf_op jit(solution)/shard_map/all_to_all | solution.py:132
  90.8 2.6 %copy.76 = bf16[12,32,2048]{2,1,0:T(8,128)(2,1)S(1)} copy(bf16[12,32,2048]{2,0,1:T(8,128)(2,1)} %all-to-all-done.1) | data formatting | bytes 3145728 | tf_op jit(solution)/shard_map/all_to_all | solution.py:132
  93.5 1.1 copy-done.2
  94.6 1.9 %fusion.4 = f32[384,512]{1,0:T(8,128)} fusion(bf16[384,2048]{1,0:T(8,128)(2,1)S(1)} %bitcast.42, bf16[1,2048,512]{2,1,0:T(8,128)(2,1)S(1)} %copy-done.21), kind=kOutput, calls=%fused_computation.8 | convolution fusion | flops 805306368 | bytes 4456448 | tf_op jit(solution)/shard_map/dot_general | solution.py:66
  96.5 5.3 %convolution_convert_fusion = bf16[384,2048]{1,0:T(8,128)(2,1)} fusion(bf16[1,512,2048]{2,1,0:T(8,128)(2,1)S(1)} %copy-done, bf16[384,2048]{1,0:T(8,128)(2,1)} %bitcast.43, bf16[1,2048,512]{2,1,0:T(8,128)(2,1)} %param.36, f32[384,512]{1,0:T(8,128)} %fusion.4), kind=kOutput, calls=%fused_computation.2 | convolution fusion | flops 1612578816 | bytes 8126464 | tf_op jit(solution)/shard_map/dot_general | solution.py:69
  101.8 3.7 %copy_select_fusion = bf16[12,32,2048]{2,0,1:T(8,128)(2,1)} fusion(bf16[12,32,2048]{2,1,0:T(8,128)(2,1)} %bitcast.44, pred[12,32]{0,1:T(8,128)(4,1)S(1)} %iota_compare_fusion.1), kind=kLoop, calls=%fused_computation.10 | loop fusion | flops 786432 | bytes 3146112 | tf_op jit(solution)/shard_map/jit(_where)/select_n | solution.py:73
  105.5 4.1 %all-to-all-start.2 = ((bf16[12,32,2048]{2,0,1:T(8,128)(2,1)}), bf16[12,32,2048]{2,0,1:T(8,128)(2,1)}, u32[]{:S(2)}, u32[]{:S(2)}) async-start(bf16[12,32,2048]{2,0,1:T(8,128)(2,1)} %copy_select_fusion), calls=%async_computation.2 | async-start | bytes 4194304 | tf_op jit(solution)/shard_map/all_to_all | solution.py:138
  109.6 0.1 mul.210
  109.8 0.1 copy.71
  110.0 0.7 copy.68
  110.7 0.8 fusion.36
  111.5 46.8 %all-to-all-done.2 = bf16[12,32,2048]{2,0,1:T(8,128)(2,1)} async-done(((bf16[12,32,2048]{2,0,1:T(8,128)(2,1)}), bf16[12,32,2048]{2,0,1:T(8,128)(2,1)}, u32[]{:S(2)}, u32[]{:S(2)}) %all-to-all-start.2) | async-done | bytes 1572896 | tf_op jit(solution)/shard_map/all_to_all | solution.py:138
  158.3 3.6 %copy.78 = bf16[12,32,2048]{2,1,0:T(8,128)(2,1)} copy(bf16[12,32,2048]{2,0,1:T(8,128)(2,1)} %all-to-all-done.2) | data formatting | bytes 3145728 | tf_op jit(solution)/shard_map/all_to_all | solution.py:138
  161.9 3.1 %gather_fusion = bf16[128,2048]{1,0:T(8,128)(2,1)S(1)} fusion(bf16[384,2048]{1,0:T(8,128)(2,1)} %bitcast.40, s32[1024]{0:T(1024)S(1)} %pad_clamp_fusion), kind=kCustom, calls=%fused_computation | custom fusion | bytes 1049088 | tf_op jit(solution)/shard_map/jit(_take)/gather | solution.py:139
  165.0 1.1 gather.7
  166.1 3.7 %multiply_reduce_fusion = f32[64,2048]{1,0:T(8,128)S(1)} fusion(bf16[64,2,2048]{2,1,0:T(2,128)(2,1)} %gather.7, pred[64,2]{1,0:T(8,128)(4,1)S(1)} %copy.71, f32[64,2]{1,0:T(8,128)S(1)} %copy-done.6), kind=kLoop, calls=%fused_computation.27 | loop fusion | flops 917504 | bytes 1049216 | tf_op jit(solution)/shard_map/reduce_sum | solution.py:142
  169.8 0.1 multiply_reduce_fusion.2
  170.0 0.9 add_convert_fusion
  (60 shorter events, 0.5 us)
Async XLA Ops:
  0.6 95.8 %copy-start = (bf16[1,512,2048]{2,1,0:T(8,128)(2,1)S(1)}, bf16[1,512,2048]{2,1,0:T(8,128)(2,1)}, u32[]{:S(2)}) copy-start(bf16[1,512,2048]{2,1,0:T(8,128)(2,1)} %param.37) | copy-start | bytes 6291460
  3.4 32.6 %all-to-all-start = ((s32[1,32,1]{2,0,1:T(1,128)}), s32[1,32,1]{2,0,1:T(1,128)S(1)}, u32[]{:S(2)}, u32[]{:S(2)}) async-start(s32[1,32,1]{2,0,1:T(1,128)} %copy.72), calls=%async_computation | async-start | bytes 32768 | tf_op jit(solution)/shard_map/all_to_all | solution.py:133
  12.5 3.3 %copy-start.16 = (f32[64]{0:T(128)}, f32[64]{0:T(128)S(1)}, u32[]{:S(2)}) copy-start(f32[64]{0:T(128)S(1)} %add_rsqrt_fusion.3) | copy-start | bytes 772
  12.5 3.3 %copy-start.3 = (bf16[64,3,1024]{2,0,1:T(8,128)(2,1)S(1)}, bf16[64,3,1024]{2,0,1:T(8,128)(2,1)}, u32[]{:S(2)}) copy-start(bf16[64,3,1024]{2,0,1:T(8,128)(2,1)} %param.20) | copy-start | bytes 1179652
  12.5 3.3 %copy-start.9 = (f32[4,1024]{1,0:T(4,128)S(1)}, f32[4,1024]{1,0:T(4,128)}, u32[]{:S(2)}) copy-start(f32[4,1024]{1,0:T(4,128)} %param.24) | copy-start | bytes 49156
  12.5 3.6 %copy-start.22 = (bf16[16,64,64]{2,1,0:T(8,128)(2,1)S(1)}, bf16[16,64,64]{2,1,0:T(8,128)(2,1)}, u32[]{:S(2)}) copy-start(bf16[16,64,64]{2,1,0:T(8,128)(2,1)} %param.25) | copy-start | bytes 393220
  18.2 3.2 %copy-start.1 = (bf16[64,2048]{1,0:T(8,128)(2,1)S(1)}, bf16[64,2048]{1,0:T(8,128)(2,1)}, u32[]{:S(2)}) copy-start(bf16[64,2048]{1,0:T(8,128)(2,1)} %param.19) | copy-start | bytes 786436
  21.3 5.4 %copy-start.5 = (f32[64,1024]{1,0:T(8,128)}, f32[64,1024]{1,0:T(8,128)S(1)}, u32[]{:S(2)}) copy-start(f32[64,1024]{1,0:T(8,128)S(1)} %multiply_add_fusion) | copy-start | bytes 786436
  21.4 5.4 %copy-start.7 = (f32[2048]{0:T(1024)S(1)}, f32[2048]{0:T(1024)}, u32[]{:S(2)}) copy-start(f32[2048]{0:T(1024)} %param.30) | copy-start | bytes 24580
  21.4 5.7 %copy-start.10 = (f32[2048]{0:T(1024)S(1)}, f32[2048]{0:T(1024)}, u32[]{:S(2)}) copy-start(f32[2048]{0:T(1024)} %param.31) | copy-start | bytes 24580
  21.4 5.9 %copy-start.17 = (s32[128]{0:T(128)S(1)}, s32[128]{0:T(128)}, u32[]{:S(2)}) copy-start(s32[128]{0:T(128)} %get-tuple-element.4) | copy-start | bytes 1540
  21.4 5.9 %copy-start.19 = (s32[128,1]{0,1:T(1,128)S(1)}, s32[128,1]{0,1:T(1,128)}, u32[]{:S(2)}) copy-start(s32[128,1]{0,1:T(1,128)} %reshape.196) | copy-start | bytes 1540
  26.8 0.5 copy-start.12
  36.0 54.8 %all-to-all-start.1 = ((bf16[12,32,2048]{2,0,1:T(8,128)(2,1)}), bf16[12,32,2048]{2,0,1:T(8,128)(2,1)}, u32[]{:S(2)}, u32[]{:S(2)}) async-start(bf16[12,32,2048]{2,0,1:T(8,128)(2,1)} %copy.75), calls=%async_computation.1 | async-start | bytes 4194304 | tf_op jit(solution)/shard_map/all_to_all | solution.py:132
  90.8 3.8 %copy-start.21 = (bf16[1,2048,512]{2,1,0:T(8,128)(2,1)S(1)}, bf16[1,2048,512]{2,1,0:T(8,128)(2,1)}, u32[]{:S(2)}) copy-start(bf16[1,2048,512]{2,1,0:T(8,128)(2,1)} %param.35) | copy-start | bytes 6291460
  93.5 1.1 copy-start.2
  105.4 4.1 %copy-start.18 = (s32[128]{0:T(128)S(1)}, s32[128]{0:T(128)}, u32[]{:S(2)}) copy-start(s32[128]{0:T(128)} %get-tuple-element.4) | copy-start | bytes 1540
  105.4 4.4 %copy-start.14 = (s32[64,2]{0,1:T(2,128)S(1)}, s32[64,2]{0,1:T(2,128)}, u32[]{:S(2)}) copy-start(s32[64,2]{0,1:T(2,128)} %param.33) | copy-start | bytes 1540
  105.4 4.5 %copy-start.15 = (f32[64,2]{0,1:T(2,128)S(1)}, f32[64,2]{0,1:T(2,128)}, u32[]{:S(2)}) copy-start(f32[64,2]{0,1:T(2,128)} %param.34) | copy-start | bytes 1540
  105.4 5.3 %copy-start.20 = (s32[128]{0:T(128)S(1)}, s32[128]{0:T(128)}, u32[]{:S(2)}) copy-start(s32[128]{0:T(128)} %fusion.57) | copy-start | bytes 1540
  105.4 5.3 %copy-start.4 = (bf16[64,3,1024]{2,0,1:T(8,128)(2,1)S(1)}, bf16[64,3,1024]{2,0,1:T(8,128)(2,1)}, u32[]{:S(2)}) copy-start(bf16[64,3,1024]{2,0,1:T(8,128)(2,1)} %param.20) | copy-start | bytes 1179652
  105.5 52.8 %all-to-all-start.2 = ((bf16[12,32,2048]{2,0,1:T(8,128)(2,1)}), bf16[12,32,2048]{2,0,1:T(8,128)(2,1)}, u32[]{:S(2)}, u32[]{:S(2)}) async-start(bf16[12,32,2048]{2,0,1:T(8,128)(2,1)} %copy_select_fusion), calls=%async_computation.2 | async-start | bytes 4194304 | tf_op jit(solution)/shard_map/all_to_all | solution.py:138
  161.9 4.2 %copy-start.6 = (f32[64,2]{1,0:T(8,128)S(1)}, f32[64,2]{1,0:T(8,128)}, u32[]{:S(2)}) copy-start(f32[64,2]{1,0:T(8,128)} %copy.68) | copy-start | bytes 1540
  165.0 5.0 %copy-start.8 = (f32[2048]{0:T(1024)S(1)}, f32[2048]{0:T(1024)}, u32[]{:S(2)}) copy-start(f32[2048]{0:T(1024)} %param.30) | copy-start | bytes 24580
  165.0 5.0 %copy-start.11 = (f32[2048]{0:T(1024)S(1)}, f32[2048]{0:T(1024)}, u32[]{:S(2)}) copy-start(f32[2048]{0:T(1024)} %param.32) | copy-start | bytes 24580
  165.0 5.0 %copy-start.13 = (f32[64]{0:T(128)S(1)}, f32[64]{0:T(128)}, u32[]{:S(2)}) copy-start(f32[64]{0:T(128)} %copy-done.12) | copy-start | bytes 772
where the time goes:
time: 172 us; the launch traced here: 171 us
  waiting for transfers between devices  94.5 us (55%)
  local copies, waits for them, and re-layouts  25.2 us (15%)
  starting transfers between devices  17.6 us (10%)
  matrix products  17.3 us (10%)
  other arithmetic  15.3 us (9%)
    all_to_all x1, waiting for transfers between devices, shards(): lax.all_to_all(outgoing, 'ep', split_axis=1, concat_axis=1, tiled=True)  47.7 us
    all_to_all x1, waiting for transfers between devices, shards(): lax.all_to_all(finished, 'ep', split_axis=1, concat_axis=1, tiled=True)  46.8 us
    all_to_all x1, starting transfers between devices, shards(): lax.all_to_all(send_info, 'ep', split_axis=1, concat_axis=1, tiled=True)  7.33 us
    all_to_all x1, starting transfers between devices, shards(): lax.all_to_all(outgoing, 'ep', split_axis=1, concat_axis=1, tiled=True)  6.14 us
    dot_general x1, matrix products, recurrence(): jnp.dot(merged, w_mix, preferred_element_type=jnp.float32)  5.34 us
    dot_general x1, matrix products, expert_block(): jnp.dot(hidden, w_expert_down[0], preferred_element_type=jnp.float32)  5.3 us
    gather x2, local copies, waits for them, and re-layouts, shards(): jnp.take(gathered.reshape(capacity * experts, model_width), slot_target,...  4.19 us
    all_to_all x1, starting transfers between devices, shards(): lax.all_to_all(finished, 'ep', split_axis=1, concat_axis=1, tiled=True)  4.11 us
  transfers between devices with their start and end apart: 3, of which 2 were waited for; matrix products, arithmetic and copies ran while one was open for 16% of the time, Pallas kernels for 0%

commit v1 on v0

--- a/solution.py
+++ b/solution.py
@@ -135,7 +135,10 @@
     finished = expert_block(
         got_rows, got_info, cap_total, w_expert_gate, w_expert_up, w_expert_down
     )
-    gathered = lax.all_to_all(finished, "ep", split_axis=1, concat_axis=1, tiled=True)
+    gathered = jnp.concatenate(
+        lax.all_to_all(jnp.stack(jnp.split(finished, lax.axis_size("ep"), axis=1)), "ep", 0, 0),
+        axis=1,
+    )
     picked = jnp.take(gathered.reshape(capacity * experts, model_width), slot_target, axis=0)
     picked = picked.astype(jnp.float32).reshape(seq_count, top_count, model_width)
     weights = affinity / jnp.sum(affinity, axis=1, keepdims=True)

time: 172 us -> 190 us (1.10)
  local copies, waits for them, and re-layouts: 25.2 us -> 45.1 us
    unnamed x47 -> x78, local copies, waits for them, and re-layouts: 2.19 us -> 21.5 us
    all_to_all x1 -> x0, local copies, waits for them, and re-layouts: 3.61 us -> none  [shards(): lax.all_to_all(finished, 'ep', split_axis=1, concat_axis=1, tiled=True)]
    reshape x0 -> x1, local copies, waits for them, and re-layouts: none -> 3.61 us  [shards(): jnp.concatenate(lax.all_to_all(jnp.stack(jnp.split(finished, lax.axis_siz...]
  transfers between devices with their start and end apart: 3 -> 3, of which waited for: 2 -> 2; matrix products, arithmetic and copies ran while one was open for 16% -> 15% of each run, Pallas kernels for 0% -> 0%
where the time goes in v1:
time: 190 us
  waiting for transfers between devices  94.5 us (50%)
  local copies, waits for them, and re-layouts  45.1 us (24%)
  starting transfers between devices  17.6 us (9%)
  matrix products  17.3 us (9%)
  other arithmetic  14 us (7%)
    all_to_all x1, waiting for transfers between devices, shards(): lax.all_to_all(outgoing, 'ep', split_axis=1, concat_axis=1, tiled=True)  47.7 us
    all_to_all x1, waiting for transfers between devices, shards(): lax.all_to_all(jnp.stack(jnp.split(finished, lax.axis_size('ep'), axis=1)...  46.8 us
    unnamed x78, local copies, waits for them, and re-layouts  21.5 us
    all_to_all x1, starting transfers between devices, shards(): lax.all_to_all(send_info, 'ep', split_axis=1, concat_axis=1, tiled=True)  7.33 us
    all_to_all x1, starting transfers between devices, shards(): lax.all_to_all(outgoing, 'ep', split_axis=1, concat_axis=1, tiled=True)  6.14 us
    dot_general x1, matrix products, recurrence(): jnp.dot(merged, w_mix, preferred_element_type=jnp.float32)  5.34 us
    dot_general x1, matrix products, expert_block(): jnp.dot(hidden, w_expert_down[0], preferred_element_type=jnp.float32)  5.3 us
    gather x2, local copies, waits for them, and re-layouts, shards(): jnp.take(gathered.reshape(capacity * experts, model_width), slot_target,...  4.19 us
  transfers between devices with their start and end apart: 3, of which 2 were waited for; matrix products, arithmetic and copies ran while one was open for 15% of the time, Pallas kernels for 0%

profile of v1, /device:TPU:0, one launch (start us, length us, event | category | flops | bytes accessed | tf_op | source)
XLA Modules:
  0.0 189.5 jit_solution(6916450896216639652)
XLA Ops:
  0.6 0.9 copy.103
  2.0 0.7 fusion.87
  2.7 0.7 copy.106
  3.4 7.3 %all-to-all-start = ((s32[1,32,1]{2,0,1:T(1,128)}), s32[1,32,1]{2,0,1:T(1,128)S(1)}, u32[]{:S(2)}, u32[]{:S(2)}) async-start(s32[1,32,1]{2,0,1:T(1,128)} %copy.106), calls=%async_computation | async-start | bytes 32768 | tf_op jit(solution)/shard_map/all_to_all | solution.py:133
  10.7 0.7 reshape.196
  11.4 1.1 fusion.31
  12.5 3.2 %fusion.21 = bf16[64,1,1024]{2,0,1:T(8,128)(2,1)S(1)} fusion(bf16[2048,1024]{1,0:T(8,128)(2,1)} %param.22, bf16[64,2048]{1,0:T(8,128)(2,1)} %param.19, f32[2048]{0:T(1024)} %param.29, f32[64]{0:T(128)S(1)} %add_rsqrt_fusion.3), kind=kOutput, calls=%fused_computation.26 | convolution fusion | flops 269025280 | bytes 4595968 | tf_op jit(solution)/shard_map/dot_general | solution.py:31
  16.9 1.2 fusion.19
  18.5 0.9 div.40
  19.4 0.7 fusion.88
  20.1 1.3 multiply_add_fusion
  21.4 5.3 %multiply_reduce_fusion.4 = (f32[64]{0:T(128)S(1)}, f32[64,2048]{1,0:T(8,128)S(1)}) fusion(bf16[1024,2048]{1,0:T(8,128)(2,1)} %param.28, f32[64,1024]{1,0:T(8,128)S(1)} %multiply_add_fusion, bf16[2048,1024]{1,0:T(8,128)(2,1)} %param.23, bf16[64,2048]{1,0:T(8,128)(2,1)S(1)} %copy-done.1, f32[2048]{0:T(1024)} %param.29, f32[64]{0:T(128)} %copy-done.16), kind=kOutput, calls=%fused_computation.50 | convolution fusion | flops 538705856 | bytes 9445888 | tf_op jit(solution)/shard_map/dot_general | solution.py:53
  28.1 1.0 reshape.214
  29.1 3.2 %scatter_custom_fusion = bf16[384,2048]{1,0:T(8,128)(2,1)} fusion(s32[128]{0:T(128)} %fusion.89, bf16[128,2048]{1,0:T(8,128)(2,1)} %reshape.214, bf16[]{:T(256)} %constant.60.clone.1), kind=kCustom, calls=%fused_computation.35 | custom fusion | bytes 1573376 | tf_op jit(solution)/shard_map/scatter | solution.py:127
  32.4 3.7 %copy.109 = bf16[12,32,2048]{2,0,1:T(8,128)(2,1)} copy(bf16[12,32,2048]{2,1,0:T(8,128)(2,1)} %bitcast.170) | data formatting | bytes 3145728 | tf_op jit(solution)/shard_map/reshape | solution.py:129
  36.0 6.1 %all-to-all-start.1 = ((bf16[12,32,2048]{2,0,1:T(8,128)(2,1)}), bf16[12,32,2048]{2,0,1:T(8,128)(2,1)}, u32[]{:S(2)}, u32[]{:S(2)}) async-start(bf16[12,32,2048]{2,0,1:T(8,128)(2,1)} %copy.109), calls=%async_computation.1 | async-start | bytes 4194304 | tf_op jit(solution)/shard_map/all_to_all | solution.py:132
  42.4 0.7 reduce
  43.1 47.7 %all-to-all-done.1 = bf16[12,32,2048]{2,0,1:T(8,128)(2,1)} async-done(((bf16[12,32,2048]{2,0,1:T(8,128)(2,1)}), bf16[12,32,2048]{2,0,1:T(8,128)(2,1)}, u32[]{:S(2)}, u32[]{:S(2)}) %all-to-all-start.1) | async-done | bytes 1572896 | tf_op jit(solution)/shard_map/all_to_all | solution.py:132
  90.8 2.6 %copy.110 = bf16[12,32,2048]{2,1,0:T(8,128)(2,1)S(1)} copy(bf16[12,32,2048]{2,0,1:T(8,128)(2,1)} %all-to-all-done.1) | data formatting | bytes 3145728 | tf_op jit(solution)/shard_map/all_to_all | solution.py:132
  93.5 1.1 copy-done.2
  94.6 1.9 fusion.4
  96.5 5.3 %convolution_convert_fusion = bf16[384,2048]{1,0:T(8,128)(2,1)} fusion(bf16[1,512,2048]{2,1,0:T(8,128)(2,1)S(1)} %copy-done, bf16[384,2048]{1,0:T(8,128)(2,1)} %bitcast.172, bf16[1,2048,512]{2,1,0:T(8,128)(2,1)} %param.36, f32[384,512]{1,0:T(8,128)} %fusion.4), kind=kOutput, calls=%fused_computation.2 | convolution fusion | flops 1612578816 | bytes 8126464 | tf_op jit(solution)/shard_map/dot_general | solution.py:69
  101.8 2.4 %copy_select_fusion = bf16[12,32,2048]{2,0,1:T(8,128)(2,1)S(1)} fusion(bf16[12,32,2048]{2,1,0:T(8,128)(2,1)} %bitcast.173, pred[12,32]{0,1:T(8,128)(4,1)S(1)} %iota_compare_fusion.1), kind=kLoop, calls=%fused_computation.10 | loop fusion | flops 786432 | bytes 3146112 | tf_op jit(solution)/shard_map/jit(_where)/select_n | solution.py:73
  104.2 0.6 fusion.85
  106.0 0.6 fusion.82
  106.6 0.6 fusion.81
  107.3 0.6 fusion.80
  108.5 0.6 fusion.78
  111.0 0.6 fusion.74
  112.9 0.6 fusion.71
  113.5 0.6 fusion.70
  114.1 0.6 fusion.69
  114.7 0.6 fusion.68
  115.4 0.6 fusion.67
  116.6 0.6 fusion.65
  117.2 0.6 fusion.64
  120.3 0.6 fusion.59
  121.0 0.6 fusion.58
  122.8 0.6 fusion.55
  124.1 4.1 %all-to-all-start.2 = ((bf16[32,12,1,2048]{3,1,2,0:T(8,128)(2,1)}), bf16[32,12,1,2048]{3,1,2,0:T(8,128)(2,1)}, u32[]{:S(2)}, u32[]{:S(2)}) async-start(bf16[32,12,1,2048]{3,1,2,0:T(8,128)(2,1)} %fusion.54), calls=%async_computation.2 | async-start | bytes 4194304 | tf_op jit(solution)/shard_map/all_to_all | solution.py:139
  128.6 0.7 copy.102
  129.3 0.8 fusion.36
  130.1 46.8 %all-to-all-done.2 = bf16[32,12,1,2048]{3,1,2,0:T(8,128)(2,1)} async-done(((bf16[32,12,1,2048]{3,1,2,0:T(8,128)(2,1)}), bf16[32,12,1,2048]{3,1,2,0:T(8,128)(2,1)}, u32[]{:S(2)}, u32[]{:S(2)}) %all-to-all-start.2) | async-done | bytes 1572896 | tf_op jit(solution)/shard_map/all_to_all | solution.py:139
  176.9 3.6 %copy.112 = bf16[12,32,1,2048]{3,1,0,2:T(8,128)(2,1)} copy(bf16[12,32,1,2048]{3,0,2,1:T(8,128)(2,1)} %bitcast.45) | data formatting | bytes 3145728 | tf_op jit(solution)/shard_map/reshape | solution.py:138
  180.5 3.1 %gather_fusion = bf16[128,2048]{1,0:T(8,128)(2,1)S(1)} fusion(bf16[384,2048]{1,0:T(8,128)(2,1)} %bitcast.169, s32[1024]{0:T(1024)S(1)} %pad_clamp_fusion), kind=kCustom, calls=%fused_computation | custom fusion | bytes 1049088 | tf_op jit(solution)/shard_map/jit(_take)/gather | solution.py:142
  183.6 1.1 gather.7
  184.7 3.7 %multiply_reduce_fusion = f32[64,2048]{1,0:T(8,128)S(1)} fusion(bf16[64,2,2048]{2,1,0:T(2,128)(2,1)} %gather.7, pred[64,2]{1,0:T(8,128)(4,1)S(1)} %copy.105, f32[64,2]{1,0:T(8,128)S(1)} %copy-done.6), kind=kLoop, calls=%fused_computation.27 | loop fusion | flops 917504 | bytes 1049216 | tf_op jit(solution)/shard_map/reduce_sum | solution.py:145
  188.6 0.9 add_convert_fusion
  (92 shorter events, 13.9 us)
Async XLA Ops:
  0.6 95.8 %copy-start = (bf16[1,512,2048]{2,1,0:T(8,128)(2,1)S(1)}, bf16[1,512,2048]{2,1,0:T(8,128)(2,1)}, u32[]{:S(2)}) copy-start(bf16[1,512,2048]{2,1,0:T(8,128)(2,1)} %param.37) | copy-start | bytes 6291460
  3.4 32.6 %all-to-all-start = ((s32[1,32,1]{2,0,1:T(1,128)}), s32[1,32,1]{2,0,1:T(1,128)S(1)}, u32[]{:S(2)}, u32[]{:S(2)}) async-start(s32[1,32,1]{2,0,1:T(1,128)} %copy.106), calls=%async_computation | async-start | bytes 32768 | tf_op jit(solution)/shard_map/all_to_all | solution.py:133
  12.5 3.3 %copy-start.16 = (f32[64]{0:T(128)}, f32[64]{0:T(128)S(1)}, u32[]{:S(2)}) copy-start(f32[64]{0:T(128)S(1)} %add_rsqrt_fusion.3) | copy-start | bytes 772
  12.5 3.3 %copy-start.3 = (bf16[64,3,1024]{2,0,1:T(8,128)(2,1)S(1)}, bf16[64,3,1024]{2,0,1:T(8,128)(2,1)}, u32[]{:S(2)}) copy-start(bf16[64,3,1024]{2,0,1:T(8,128)(2,1)} %param.20) | copy-start | bytes 1179652
  12.5 3.3 %copy-start.9 = (f32[4,1024]{1,0:T(4,128)S(1)}, f32[4,1024]{1,0:T(4,128)}, u32[]{:S(2)}) copy-start(f32[4,1024]{1,0:T(4,128)} %param.24) | copy-start | bytes 49156
  12.5 3.6 %copy-start.22 = (bf16[16,64,64]{2,1,0:T(8,128)(2,1)S(1)}, bf16[16,64,64]{2,1,0:T(8,128)(2,1)}, u32[]{:S(2)}) copy-start(bf16[16,64,64]{2,1,0:T(8,128)(2,1)} %param.25) | copy-start | bytes 393220
  18.2 3.2 %copy-start.1 = (bf16[64,2048]{1,0:T(8,128)(2,1)S(1)}, bf16[64,2048]{1,0:T(8,128)(2,1)}, u32[]{:S(2)}) copy-start(bf16[64,2048]{1,0:T(8,128)(2,1)} %param.19) | copy-start | bytes 786436
  21.3 5.4 %copy-start.5 = (f32[64,1024]{1,0:T(8,128)}, f32[64,1024]{1,0:T(8,128)S(1)}, u32[]{:S(2)}) copy-start(f32[64,1024]{1,0:T(8,128)S(1)} %multiply_add_fusion) | copy-start | bytes 786436
  21.4 5.4 %copy-start.7 = (f32[2048]{0:T(1024)S(1)}, f32[2048]{0:T(1024)}, u32[]{:S(2)}) copy-start(f32[2048]{0:T(1024)} %param.30) | copy-start | bytes 24580
  21.4 5.7 %copy-start.10 = (f32[2048]{0:T(1024)S(1)}, f32[2048]{0:T(1024)}, u32[]{:S(2)}) copy-start(f32[2048]{0:T(1024)} %param.31) | copy-start | bytes 24580
  21.4 5.9 %copy-start.17 = (s32[128]{0:T(128)S(1)}, s32[128]{0:T(128)}, u32[]{:S(2)}) copy-start(s32[128]{0:T(128)} %get-tuple-element.4) | copy-start | bytes 1540
  21.4 5.9 %copy-start.19 = (s32[128,1]{0,1:T(1,128)S(1)}, s32[128,1]{0,1:T(1,128)}, u32[]{:S(2)}) copy-start(s32[128,1]{0,1:T(1,128)} %reshape.196) | copy-start | bytes 1540
  26.8 0.5 copy-start.12
  36.0 54.8 %all-to-all-start.1 = ((bf16[12,32,2048]{2,0,1:T(8,128)(2,1)}), bf16[12,32,2048]{2,0,1:T(8,128)(2,1)}, u32[]{:S(2)}, u32[]{:S(2)}) async-start(bf16[12,32,2048]{2,0,1:T(8,128)(2,1)} %copy.109), calls=%async_computation.1 | async-start | bytes 4194304 | tf_op jit(solution)/shard_map/all_to_all | solution.py:132
  90.8 3.8 %copy-start.21 = (bf16[1,2048,512]{2,1,0:T(8,128)(2,1)S(1)}, bf16[1,2048,512]{2,1,0:T(8,128)(2,1)}, u32[]{:S(2)}) copy-start(bf16[1,2048,512]{2,1,0:T(8,128)(2,1)} %param.35) | copy-start | bytes 6291460
  93.5 1.2 copy-start.2
  124.1 4.1 %copy-start.18 = (s32[128]{0:T(128)S(1)}, s32[128]{0:T(128)}, u32[]{:S(2)}) copy-start(s32[128]{0:T(128)} %get-tuple-element.4) | copy-start | bytes 1540
  124.1 4.3 %copy-start.14 = (s32[64,2]{0,1:T(2,128)S(1)}, s32[64,2]{0,1:T(2,128)}, u32[]{:S(2)}) copy-start(s32[64,2]{0,1:T(2,128)} %param.33) | copy-start | bytes 1540
  124.1 4.5 %copy-start.15 = (f32[64,2]{0,1:T(2,128)S(1)}, f32[64,2]{0,1:T(2,128)}, u32[]{:S(2)}) copy-start(f32[64,2]{0,1:T(2,128)} %param.34) | copy-start | bytes 1540
  124.1 5.2 %copy-start.20 = (s32[128]{0:T(128)S(1)}, s32[128]{0:T(128)}, u32[]{:S(2)}) copy-start(s32[128]{0:T(128)} %fusion.89) | copy-start | bytes 1540
  124.1 5.3 %copy-start.4 = (bf16[64,3,1024]{2,0,1:T(8,128)(2,1)S(1)}, bf16[64,3,1024]{2,0,1:T(8,128)(2,1)}, u32[]{:S(2)}) copy-start(bf16[64,3,1024]{2,0,1:T(8,128)(2,1)} %param.20) | copy-start | bytes 1179652
  124.1 52.8 %all-to-all-start.2 = ((bf16[32,12,1,2048]{3,1,2,0:T(8,128)(2,1)}), bf16[32,12,1,2048]{3,1,2,0:T(8,128)(2,1)}, u32[]{:S(2)}, u32[]{:S(2)}) async-start(bf16[32,12,1,2048]{3,1,2,0:T(8,128)(2,1)} %fusion.54), calls=%async_computation.2 | async-start | bytes 4194304 | tf_op jit(solution)/shard_map/all_to_all | solution.py:139
  180.5 4.2 %copy-start.6 = (f32[64,2]{1,0:T(8,128)S(1)}, f32[64,2]{1,0:T(8,128)}, u32[]{:S(2)}) copy-start(f32[64,2]{1,0:T(8,128)} %copy.102) | copy-start | bytes 1540
  183.6 5.0 %copy-start.8 = (f32[2048]{0:T(1024)S(1)}, f32[2048]{0:T(1024)}, u32[]{:S(2)}) copy-start(f32[2048]{0:T(1024)} %param.30) | copy-start | bytes 24580
  183.6 5.0 %copy-start.11 = (f32[2048]{0:T(1024)S(1)}, f32[2048]{0:T(1024)}, u32[]{:S(2)}) copy-start(f32[2048]{0:T(1024)} %param.32) | copy-start | bytes 24580
  183.6 5.0 %copy-start.13 = (f32[64]{0:T(128)S(1)}, f32[64]{0:T(128)}, u32[]{:S(2)}) copy-start(f32[64]{0:T(128)} %copy-done.12) | copy-start | bytes 772
